TPU v7x, 32 devices: a whole 2x2x4 slice. The times are simulated.
32 devices in a mesh: rep: 2 (over x), fs: 8 (over z, y), tp: 2 (over core).
Axes of the slice: x: 2, y: 2, z: 4, core: 2. Of those that a mesh axis runs over, the one named last changes fastest.
Arguments:
- tokens: bfloat16 [4096, 1024], P(('rep', 'fs', 'tp')), may hold values from -4 to 4
- mixer_out: bfloat16 [4096, 1024], P(('rep', 'fs')), may hold values from -4 to 4
- gain_first: float32 [1024], replicated, may hold values from 0.1 to 1.9
- gate_first: bfloat16 [1024, 2816], P('fs', 'tp'), may hold values from -0.1875 to 0.1875
- up_first: bfloat16 [1024, 2816], P('fs', 'tp'), may hold values from -0.1875 to 0.1875
- down_first: bfloat16 [2816, 1024], P('tp', 'fs'), may hold values from -0.109375 to 0.109375
- gain_second: float32 [1024], replicated, may hold values from 0.1 to 1.9
- gate_second: bfloat16 [1024, 2816], P('fs', 'tp'), may hold values from -0.1875 to 0.1875
- up_second: bfloat16 [1024, 2816], P('fs', 'tp'), may hold values from -0.1875 to 0.1875
- down_second: bfloat16 [2816, 1024], P('tp', 'fs'), may hold values from -0.109375 to 0.109375
- gain_last: float32 [1024], P('tp'), may hold values from 0.1 to 1.9
Outputs:
- result: bfloat16 [4096, 1024], P(('rep', 'fs'), 'tp')
All inputs are finite; a program needn't handle non-finite values.
Results may differ from a plain program's by a relative error of at most 0.02.
Values may be sent and summed in bfloat16 or wider, within the bound.
A program may use at most 64 MiB of HBM per device.

v0:
```python
import jax
import jax.numpy as jnp
from jax import lax
from jax.sharding import PartitionSpec as P

EPS = 1e-06


def over_all(slab, axis, dim):

    def gathered(part):
        return lax.all_gather(part, axis, axis=dim, tiled=True)

    return jax.tree.map(gathered, slab)


def normalize(floats_in, gain_vec):
    floats = floats_in.astype(jnp.float32)
    factor = lax.rsqrt(jnp.mean(floats * floats, axis=-1, keepdims=True) + EPS)
    return (floats * factor * gain_vec.astype(jnp.float32)).astype(jnp.bfloat16)


def gather_group(row_block):
    return lax.all_gather(row_block, "tp", axis=0, tiled=True)


def inner_hidden(normed, w_gate, w_up):

    def add_both(totals, pieces):
        columns = lax.slice_in_dim(normed, 0, pieces[0].shape[0], axis=1)
        return (
            totals[0] + jnp.dot(columns, pieces[0], preferred_element_type=jnp.float32),
            totals[1] + jnp.dot(columns, pieces[1], preferred_element_type=jnp.float32),
        )

    empty = jnp.zeros((normed.shape[0], w_gate.shape[1]), jnp.float32)
    gate_acc, up_acc = add_both((empty, empty), over_all((w_gate, w_up), "fs", 0))
    return (jax.nn.silu(gate_acc) * up_acc).astype(jnp.bfloat16)


def outer_weight(w_down):
    return lax.all_gather(w_down, "fs", axis=1, tiled=True)


def local(
    tokens,
    mixer_out,
    gain_first,
    gate_first,
    up_first,
    down_first,
    gain_second,
    gate_second,
    up_second,
    down_second,
    gain_last,
):
    rows_dev = tokens.shape[0]
    tp_count = lax.axis_size("tp")
    tp_index = lax.axis_index("tp")
    normed_own = normalize(tokens, gain_first)
    normed_one = gather_group(normed_own)
    hidden_one = inner_hidden(normed_one, gate_first, up_first)
    down_full = outer_weight(down_first)

    def row_terms():
        picked = lax.slice_in_dim(hidden_one, 0, rows_dev * lax.axis_size("tp"), axis=0)
        return jnp.dot(picked, down_full, preferred_element_type=jnp.float32)

    ffn_one = lax.psum_scatter(
        row_terms().astype(jnp.bfloat16), "tp", scatter_dimension=0, tiled=True
    ).astype(jnp.float32)
    after_one = (tokens.astype(jnp.float32) + 0.5 * ffn_one).astype(jnp.bfloat16)
    own_mixer = lax.dynamic_slice_in_dim(mixer_out, tp_index * rows_dev, rows_dev, 0)
    mixed_in = (after_one.astype(jnp.float32) + own_mixer.astype(jnp.float32)).astype(jnp.bfloat16)
    gathered = gather_group(mixed_in)
    normed_two = normalize(gathered, gain_second)
    hidden_two = inner_hidden(normed_two, gate_second, up_second)
    down_two_full = outer_weight(down_second)
    terms_two = jnp.dot(hidden_two, down_two_full, preferred_element_type=jnp.float32)
    ffn_two = lax.psum_scatter(
        terms_two.astype(jnp.bfloat16), "tp", scatter_dimension=1, tiled=True
    ).astype(jnp.float32)
    col_width = ffn_two.shape[1]
    my_cols = lax.dynamic_slice_in_dim(gathered, tp_index * col_width, col_width, 1)
    after_two = (my_cols.astype(jnp.float32) + 0.5 * ffn_two).astype(jnp.bfloat16)
    floats = after_two.astype(jnp.float32)
    sum_sq = lax.psum(jnp.sum(floats * floats, axis=1), "tp")
    factor = lax.rsqrt(sum_sq / (col_width * tp_count) + EPS)
    return (floats * factor[:, None] * gain_last.astype(jnp.float32)[None, :]).astype(jnp.bfloat16)


def solution(mesh):
    in_specs = (
        P(("rep", "fs", "tp"), None),
        P(("rep", "fs"), None),
        P(),
        P("fs", "tp"),
        P("fs", "tp"),
        P("tp", "fs"),
        P(),
        P("fs", "tp"),
        P("fs", "tp"),
        P("tp", "fs"),
        P("tp"),
    )
    out_specs = P(("rep", "fs"), "tp")
    return jax.shard_map(local, mesh=mesh, in_specs=in_specs, out_specs=out_specs, check_vma=False)
```

profile of v0, /device:TPU:0, one launch (start us, length us, event | category | flops | bytes accessed | tf_op | source)
XLA Modules:
  0.0 402.3 jit_solution(16282262251810732455)
XLA Ops:
  6.5 0.7 all-gather.7.cloned.1.call-update
  7.3 0.7 all-gather.11.cloned.1.call-update
  8.0 0.0 all-gather.9.cloned.1.call-start
  8.1 0.7 all-gather.9.cloned.1.call-update
  8.7 0.0 reduce-scatter.3.cloned.1.call-start
  8.8 1.1 fusion.10
  9.9 1.1 fusion.12
  11.0 2.3 all_gather.24
  13.3 56.3 %all-gather.7.cloned.1.call-done = bf16[1024,1408]{1,0:T(8,128)(2,1)} async-done(((bf16[128,1408]{1,0:T(8,128)(2,1)}), bf16[1024,1408]{1,0:T(8,128)(2,1)}) %all-gather.7.cloned.1.call-update) | async-done | bytes 2883600 | tf_op jit(solution)/shard_map/all_gather | solution.py:12
  69.6 2.8 fusion.20
  72.4 57.4 %all-gather.11.cloned.1.call-done = bf16[1408,1024]{1,0:T(8,128)(2,1)} async-done(((bf16[1408,128]{1,0:T(8,128)(2,1)}), bf16[1408,1024]{1,0:T(8,128)(2,1)}) %all-gather.11.cloned.1.call-update) | async-done | bytes 2883600 | tf_op jit(solution)/shard_map/all_gather | solution.py:42
  129.8 57.7 %all-gather.9.cloned.1.call-done = bf16[1024,1408]{1,0:T(8,128)(2,1)} async-done(((bf16[128,1408]{1,0:T(8,128)(2,1)}), bf16[1024,1408]{1,0:T(8,128)(2,1)}) %all-gather.9.cloned.1.call-update) | async-done | bytes 2883600 | tf_op jit(solution)/shard_map/all_gather | solution.py:12
  187.5 5.4 %convolution_convert_fusion.1 = bf16[256,1024]{1,0:T(8,128)(2,1)} fusion(bf16[1408,1024]{1,0:T(8,128)(2,1)} %all-gather.11.cloned.1.call-done, bf16[256,1024]{1,0:T(8,128)(2,1)S(1)} %all_gather.24, bf16[1024,1408]{1,0:T(8,128)(2,1)} %all-gather.9.cloned.1.call-done, f32[256,1408]{1,0:T(8,128)S(1)} %fusion.20), kind=kOutput, calls=%fused_computation.7 | convolution fusion | flops 1478819840 | bytes 8257536 | tf_op jit(solution)/shard_map/dot_general | solution.py:68
  193.0 0.0 all-gather.13.cloned.1.call-start
  193.0 0.5 all-gather.13.cloned.1.call-update
  193.5 0.0 all-gather.15.cloned.1.call-start
  193.6 0.5 all-gather.15.cloned.1.call-update
  194.2 0.7 all-gather.17.cloned.1.call-update
  194.9 0.0 reduce-scatter.5.cloned.1.call-start
  194.9 4.7 %reduce-scatter.3.cloned.1.call-done = bf16[128,1024]{1,0:T(8,128)(2,1)} async-done(((bf16[256,1024]{1,0:T(8,128)(2,1)}), bf16[128,1024]{1,0:T(8,128)(2,1)}) %reduce-scatter.3.cloned.1.call-update) | async-done | bytes 262160 | tf_op jit(solution)/shard_map/reduce_scatter | solution.py:70
  199.7 1.1 add_convert_fusion.1
  200.7 2.2 all_gather.28
  202.9 0.2 fusion.2
  203.1 57.0 %all-gather.13.cloned.1.call-done = bf16[1024,1408]{1,0:T(8,128)(2,1)} async-done(((bf16[128,1408]{1,0:T(8,128)(2,1)}), bf16[1024,1408]{1,0:T(8,128)(2,1)}) %all-gather.13.cloned.1.call-update) | async-done | bytes 2883600 | tf_op jit(solution)/shard_map/all_gather | solution.py:12
  260.2 2.9 fusion.16
  263.0 55.1 %all-gather.15.cloned.1.call-done = bf16[1024,1408]{1,0:T(8,128)(2,1)} async-done(((bf16[128,1408]{1,0:T(8,128)(2,1)}), bf16[1024,1408]{1,0:T(8,128)(2,1)}) %all-gather.15.cloned.1.call-update) | async-done | bytes 2883600 | tf_op jit(solution)/shard_map/all_gather | solution.py:12
  318.1 60.3 %all-gather.17.cloned.1.call-done = bf16[1408,1024]{1,0:T(8,128)(2,1)} async-done(((bf16[1408,128]{1,0:T(8,128)(2,1)}), bf16[1408,1024]{1,0:T(8,128)(2,1)}) %all-gather.17.cloned.1.call-update) | async-done | bytes 2883600 | tf_op jit(solution)/shard_map/all_gather | solution.py:42
  378.4 5.4 %convolution_convert_fusion = bf16[256,1024]{1,0:T(8,128)(2,1)} fusion(bf16[1408,1024]{1,0:T(8,128)(2,1)} %all-gather.17.cloned.1.call-done, bf16[1024,1408]{1,0:T(8,128)(2,1)} %all-gather.15.cloned.1.call-done, f32[256,1408]{1,0:T(8,128)S(1)} %fusion.16, bf16[256,1024]{1,0:T(8,128)(2,1)S(1)} %all_gather.28, f32[1024]{0:T(1024)S(1)} %copy-done.2, ...), kind=kOutput, calls=%fused_computation.6 | convolution fusion | flops 1479868416 | bytes 8262656 | tf_op jit(solution)/shard_map/dot_general | solution.py:80
  383.8 6.3 %reduce-scatter.5.cloned.1.call-done = bf16[256,512]{1,0:T(8,128)(2,1)} async-done(((bf16[256,1024]{1,0:T(8,128)(2,1)}), bf16[256,512]{1,0:T(8,128)(2,1)}) %reduce-scatter.5.cloned.1.call-update) | async-done | bytes 262160 | tf_op jit(solution)/shard_map/reduce_scatter | solution.py:81
  390.1 1.1 fusion.7
  391.2 2.5 psum.7
  393.7 1.8 fusion.9
  (16 shorter events, 0.2 us)
Async XLA Ops:
  6.5 63.0 %all-gather.7.cloned.1.call-start = ((), (), s32[]{:S(2)}) async-start(), calls=%async_computation.2 | async-start | bytes 3244032 | tf_op jit(solution)/shard_map/all_gather | solution.py:12
  7.3 122.6 %all-gather.11.cloned.1.call-start = ((), (), s32[]{:S(2)}) async-start(), calls=%async_computation.4 | async-start | bytes 3244032 | tf_op jit(solution)/shard_map/all_gather | solution.py:42
  8.0 179.5 %all-gather.9.cloned.1.call-start = ((), (), s32[]{:S(2)}) async-start(), calls=%async_computation.3 | async-start | bytes 3244032 | tf_op jit(solution)/shard_map/all_gather | solution.py:12
  8.7 190.9 %reduce-scatter.3.cloned.1.call-start = ((), (), s32[]{:S(2)}) async-start(), calls=%async_computation.5 | async-start | bytes 786432 | tf_op jit(solution)/shard_map/reduce_scatter | solution.py:70
  72.4 127.3 %copy-start = (bf16[128,1024]{1,0:T(8,128)(2,1)S(1)}, bf16[128,1024]{1,0:T(8,128)(2,1)}, u32[]{:S(2)}) copy-start(bf16[128,1024]{1,0:T(8,128)(2,1)} %param.11) | copy-start | bytes 786436
  72.4 127.3 %copy-start.1 = (bf16[256,1024]{1,0:T(8,128)(2,1)S(1)}, bf16[256,1024]{1,0:T(8,128)(2,1)}, u32[]{:S(2)}) copy-start(bf16[256,1024]{1,0:T(8,128)(2,1)} %param.12) | copy-start | bytes 1572868
  192.9 67.2 %copy-start.2 = (f32[1024]{0:T(1024)S(1)}, f32[1024]{0:T(1024)}, u32[]{:S(2)}) copy-start(f32[1024]{0:T(1024)} %param.17) | copy-start | bytes 12292
  193.0 67.2 %all-gather.13.cloned.1.call-start = ((), (), s32[]{:S(2)}) async-start(), calls=%async_computation.6 | async-start | bytes 3244032 | tf_op jit(solution)/shard_map/all_gather | solution.py:12
  193.5 124.6 %all-gather.15.cloned.1.call-start = ((), (), s32[]{:S(2)}) async-start(), calls=%async_computation.7 | async-start | bytes 3244032 | tf_op jit(solution)/shard_map/all_gather | solution.py:12
  194.1 184.3 %all-gather.17.cloned.1.call-start = ((), (), s32[]{:S(2)}) async-start(), calls=%async_computation.8 | async-start | bytes 3244032 | tf_op jit(solution)/shard_map/all_gather | solution.py:42
  194.9 195.2 %reduce-scatter.5.cloned.1.call-start = ((), (), s32[]{:S(2)}) async-start(), calls=%async_computation.9 | async-start | bytes 786432 | tf_op jit(solution)/shard_map/reduce_scatter | solution.py:81
  263.0 130.7 %copy-start.3 = (f32[512]{0:T(512)S(1)}, f32[512]{0:T(512)}, u32[]{:S(2)}) copy-start(f32[512]{0:T(512)} %param.21) | copy-start | bytes 6148
Sparse Core Ops, SparseCore 0:
  9.5 60.0 all-gather.6
  71.6 58.1 all-gather.10
  132.0 55.4 all-gather.8
  193.1 6.5 reduce-scatter.2
  201.7 58.4 all-gather.12
  262.2 55.9 all-gather.14
  320.2 58.1 all-gather.16
  384.0 6.0 reduce-scatter.4
where the time goes:
time: 403 us; the launch traced here: 402 us
  waiting for transfers between devices  359 us (89%)
  matrix products  16.5 us (4%)
  between operations  13.6 us (3%)
  blocking collectives  6.95 us (2%)
  other arithmetic  6.36 us (2%)
    all_gather x4, waiting for transfers between devices, gathered(): return lax.all_gather(part, axis, axis=dim, tiled=True)  226 us
    all_gather x2, waiting for transfers between devices, outer_weight(): return lax.all_gather(w_down, 'fs', axis=1, tiled=True)  118 us
  transfers between devices with their start and end apart: 8, of which 8 were waited for; matrix products, arithmetic and copies ran while one was open for 2% of the time, Pallas kernels for 0%

commit v1 on v0

--- a/solution.py
+++ b/solution.py
@@ -1,9 +1,40 @@
+import functools
 import jax
 import jax.numpy as jnp
 from jax import lax
 from jax.sharding import PartitionSpec as P
 
 EPS = 1e-06
+
+
+def start_ports(piece_in, named_axis):
+    seen_now, current_value, newest = (
+        lax.axis_size(named_axis),
+        lax.axis_index(named_axis),
+        piece_in.shape[1],
+    )
+    by_place = [(t, (t + 1) % seen_now) for t in range(seen_now)]
+    log = [(t, (t - 1) % seen_now) for t in range(seen_now)]
+    b_now = jnp.zeros((*piece_in.shape[:1], seen_now * newest, *piece_in.shape[2:]), piece_in.dtype)
+    b_now = lax.dynamic_update_slice_in_dim(b_now, piece_in, current_value * newest, axis=1)
+    mixed_arr = aux = piece_in
+    passed = seen_now // 2
+    dev = 1
+    while dev < passed + 1:
+        mixed_arr = lax.ppermute(mixed_arr, named_axis, by_place)
+        b_now = lax.dynamic_update_slice_in_dim(
+            b_now, mixed_arr, (current_value - dev) % seen_now * newest, axis=1
+        )
+        if dev < seen_now - passed:
+            aux = lax.ppermute(aux, named_axis, log)
+            b_now = lax.dynamic_update_slice_in_dim(
+                b_now, aux, (current_value + dev) % seen_now * newest, axis=1
+            )
+        dev += 1
+    return b_now
+
+
+_bind_slots = functools.partial(start_ports, named_axis="fs")
 
 
 def over_all(slab, axis, dim):
@@ -39,7 +70,7 @@
 
 
 def outer_weight(w_down):
-    return lax.all_gather(w_down, "fs", axis=1, tiled=True)
+    return _bind_slots(w_down)
 
 
 def local(

time: 403 us -> 337 us (0.84)
  waiting for transfers between devices: 359 us -> 248 us
  starting transfers between devices: 0.27 us -> 36.8 us
  local copies, waits for them, and re-layouts: 0.02 us -> 6.58 us
    all_gather x2 -> x0, waiting for transfers between devices: 118 us -> none  [outer_weight(): return lax.all_gather(w_down, 'fs', axis=1, tiled=True)]
    ppermute x0 -> x14, waiting for transfers between devices: none -> 106 us  [the longest x8 83.6 us: start_ports(): mixed_arr = lax.ppermute(mixed_arr, named_axis, by_place)]
    all_gather x4, waiting for transfers between devices: 226 us -> 133 us  [gathered(): return lax.all_gather(part, axis, axis=dim, tiled=True)]
    ppermute x0 -> x14, starting transfers between devices: none -> 36.6 us  [the longest x6 23.8 us: start_ports(): aux = lax.ppermute(aux, named_axis, log)]
    dynamic_update_slice x0 -> x16, local copies, waits for them, and re-layouts: none -> 5.85 us  [the longest x8 2.9 us: start_ports(): lax.dynamic_update_slice_in_dim(b_now, mixed_arr, (current_value - dev) %...]
    reduce_scatter x1, waiting for transfers between devices: 4.74 us -> 0.02 us  [local(): lax.psum_scatter(row_terms().astype(jnp.bfloat16), 'tp', scatter_dimensio...]
  transfers between devices with their start and end apart: 8 -> 20, of which waited for: 8 -> 17; matrix products, arithmetic and copies ran while one was open for 2% -> 5% of each run, Pallas kernels for 0% -> 0%
where the time goes in v1:
time: 337 us; the launch traced here: 336 us
  waiting for transfers between devices  248 us (74%)
  starting transfers between devices  36.8 us (11%)
  matrix products  17.7 us (5%)
  between operations  13.7 us (4%)
  blocking collectives  6.83 us (2%)
  local copies, waits for them, and re-layouts  6.58 us (2%)
  other arithmetic  6.5 us (2%)
    all_gather x4, waiting for transfers between devices, gathered(): return lax.all_gather(part, axis, axis=dim, tiled=True)  133 us
    ppermute x8, waiting for transfers between devices, start_ports(): mixed_arr = lax.ppermute(mixed_arr, named_axis, by_place)  83.6 us
    ppermute x6, starting transfers between devices, start_ports(): aux = lax.ppermute(aux, named_axis, log)  23.8 us
    ppermute x6, waiting for transfers between devices, start_ports(): aux = lax.ppermute(aux, named_axis, log)  22.7 us
    ppermute x8, starting transfers between devices, start_ports(): mixed_arr = lax.ppermute(mixed_arr, named_axis, by_place)  12.8 us
    dot_general x2, matrix products, add_both(): jnp.dot(columns, pieces[0], preferred_element_type=jnp.float32)  7.89 us
  transfers between devices with their start and end apart: 20, of which 17 were waited for; matrix products, arithmetic and copies ran while one was open for 5% of the time, Pallas kernels for 0%

profile of v1, /device:TPU:0, one launch (start us, length us, event | category | flops | bytes accessed | tf_op | source)
XLA Modules:
  0.0 336.2 jit_solution(15648035602739374002)
XLA Ops:
  8.1 3.0 collective-permute-start
  11.1 3.1 collective-permute-start.1
  16.4 2.2 all_gather.18
  19.1 11.5 %collective-permute-done = bf16[1408,128]{1,0:T(8,128)(2,1)} collective-permute-done((bf16[1408,128]{1,0:T(8,128)(2,1)}, bf16[1408,128]{1,0:T(8,128)(2,1)}, u32[]{:S(2)}, u32[]{:S(2)}) %collective-permute-start) | collective-permute-done | bytes 360480 | tf_op jit(solution)/shard_map/ppermute | solution.py:24
  30.7 2.5 collective-permute-start.2
  33.2 3.0 collective-permute-start.3
  38.4 10.2 %collective-permute-done.2 = bf16[1408,128]{1,0:T(8,128)(2,1)S(1)} collective-permute-done((bf16[1408,128]{1,0:T(8,128)(2,1)}, bf16[1408,128]{1,0:T(8,128)(2,1)S(1)}, u32[]{:S(2)}, u32[]{:S(2)}) %collective-permute-start.2) | collective-permute-done | bytes 360480 | tf_op jit(solution)/shard_map/ppermute | solution.py:24
  50.4 9.3 %collective-permute-start.5 = (bf16[1408,128]{1,0:T(8,128)(2,1)S(1)}, bf16[1408,128]{1,0:T(8,128)(2,1)S(1)}, u32[]{:S(2)}, u32[]{:S(2)}) collective-permute-start(bf16[1408,128]{1,0:T(8,128)(2,1)S(1)} %collective-permute-done.3), channel_id=1, source_target_pairs={{0,14},{2,0},{4,2},{6,4},{8,6},{10,8},{12,10},{14,12},{1,15},{3,1}... | collective-permute-start | bytes 1081352 | tf_op jit(solution)/shard_map/ppermute | solution.py:29
  60.0 13.2 %collective-permute-done.4 = bf16[1408,128]{1,0:T(8,128)(2,1)S(1)} collective-permute-done((bf16[1408,128]{1,0:T(8,128)(2,1)S(1)}, bf16[1408,128]{1,0:T(8,128)(2,1)S(1)}, u32[]{:S(2)}, u32[]{:S(2)}) %collective-permute-start.4) | collective-permute-done | bytes 360480 | tf_op jit(solution)/shard_map/ppermute | solution.py:24
  73.2 2.5 collective-permute-start.6
  75.8 2.3 collective-permute-done.5
  78.3 9.0 %collective-permute-done.6 = bf16[1408,128]{1,0:T(8,128)(2,1)S(1)} collective-permute-done((bf16[1408,128]{1,0:T(8,128)(2,1)S(1)}, bf16[1408,128]{1,0:T(8,128)(2,1)S(1)}, u32[]{:S(2)}, u32[]{:S(2)}) %collective-permute-start.6) | collective-permute-done | bytes 360480 | tf_op jit(solution)/shard_map/ppermute | solution.py:24
  87.4 13.1 %all-gather.5.cloned.1.call-done = bf16[1024,1408]{1,0:T(8,128)(2,1)} async-done(((bf16[128,1408]{1,0:T(8,128)(2,1)}), bf16[1024,1408]{1,0:T(8,128)(2,1)}) %all-gather.5.cloned.1.call-update) | async-done | bytes 2883600 | tf_op jit(solution)/shard_map/all_gather | solution.py:43
  100.5 3.9 %fusion.20 = f32[256,1408]{1,0:T(8,128)} fusion(bf16[256,1024]{1,0:T(8,128)(2,1)S(1)} %all_gather.18, bf16[1024,1408]{1,0:T(8,128)(2,1)} %all-gather.5.cloned.1.call-done), kind=kOutput, calls=%fused_computation.49 | convolution fusion | flops 738197504 | bytes 4849664 | tf_op jit(solution)/shard_map/dot_general | solution.py:63
  104.4 54.4 %all-gather.7.cloned.1.call-done = bf16[1024,1408]{1,0:T(8,128)(2,1)} async-done(((bf16[128,1408]{1,0:T(8,128)(2,1)}), bf16[1024,1408]{1,0:T(8,128)(2,1)}) %all-gather.7.cloned.1.call-update) | async-done | bytes 2883600 | tf_op jit(solution)/shard_map/all_gather | solution.py:43
  158.8 4.9 %convolution_convert_fusion.1 = bf16[256,1024]{1,0:T(8,128)(2,1)} fusion(bf16[1408,1024]{1,0:T(8,128)(2,1)S(1)} %constant_dynamic-update-slice_fusion.8, bf16[256,1024]{1,0:T(8,128)(2,1)S(1)} %all_gather.18, bf16[1024,1408]{1,0:T(8,128)(2,1)} %all-gather.7.cloned.1.call-done, f32[256,1408]{1,0:T(8,128)} %fusion.20), kind=kOutput, calls=%fused_computation.7 | convolution fusion | flops 1478819840 | bytes 8257536 | tf_op jit(solution)/shard_map/dot_general | solution.py:99
  165.5 4.2 %collective-permute-start.8 = (bf16[1408,128]{1,0:T(8,128)(2,1)}, bf16[1408,128]{1,0:T(8,128)(2,1)}, u32[]{:S(2)}, u32[]{:S(2)}) collective-permute-start(bf16[1408,128]{1,0:T(8,128)(2,1)} %param.20), channel_id=1, source_target_pairs={{0,14},{2,0},{4,2},{6,4},{8,6},{10,8},{12,10},{14,12},{1,15},{3,1}... | collective-permute-start | bytes 1081352 | tf_op jit(solution)/shard_map/ppermute | solution.py:29
  170.2 9.3 %collective-permute-done.7 = bf16[1408,128]{1,0:T(8,128)(2,1)} collective-permute-done((bf16[1408,128]{1,0:T(8,128)(2,1)}, bf16[1408,128]{1,0:T(8,128)(2,1)}, u32[]{:S(2)}, u32[]{:S(2)}) %collective-permute-start.7) | collective-permute-done | bytes 360480 | tf_op jit(solution)/shard_map/ppermute | solution.py:24
  179.6 2.5 collective-permute-start.9
  187.1 10.7 %collective-permute-done.9 = bf16[1408,128]{1,0:T(8,128)(2,1)S(1)} collective-permute-done((bf16[1408,128]{1,0:T(8,128)(2,1)}, bf16[1408,128]{1,0:T(8,128)(2,1)S(1)}, u32[]{:S(2)}, u32[]{:S(2)}) %collective-permute-start.9) | collective-permute-done | bytes 360480 | tf_op jit(solution)/shard_map/ppermute | solution.py:24
  197.8 5.8 %collective-permute-done.10 = bf16[1408,128]{1,0:T(8,128)(2,1)S(1)} collective-permute-done((bf16[1408,128]{1,0:T(8,128)(2,1)}, bf16[1408,128]{1,0:T(8,128)(2,1)S(1)}, u32[]{:S(2)}, u32[]{:S(2)}) %collective-permute-start.10) | collective-permute-done | bytes 360480 | tf_op jit(solution)/shard_map/ppermute | solution.py:29
  203.6 2.1 collective-permute-start.12
  206.0 10.5 %collective-permute-done.11 = bf16[1408,128]{1,0:T(8,128)(2,1)S(1)} collective-permute-done((bf16[1408,128]{1,0:T(8,128)(2,1)S(1)}, bf16[1408,128]{1,0:T(8,128)(2,1)S(1)}, u32[]{:S(2)}, u32[]{:S(2)}) %collective-permute-start.11) | collective-permute-done | bytes 360480 | tf_op jit(solution)/shard_map/ppermute | solution.py:24
  216.6 13.7 %collective-permute-done.12 = bf16[1408,128]{1,0:T(8,128)(2,1)S(1)} collective-permute-done((bf16[1408,128]{1,0:T(8,128)(2,1)S(1)}, bf16[1408,128]{1,0:T(8,128)(2,1)S(1)}, u32[]{:S(2)}, u32[]{:S(2)}) %collective-permute-start.12) | collective-permute-done | bytes 360480 | tf_op jit(solution)/shard_map/ppermute | solution.py:29
  230.4 9.1 %collective-permute-done.13 = bf16[1408,128]{1,0:T(8,128)(2,1)S(1)} collective-permute-done((bf16[1408,128]{1,0:T(8,128)(2,1)S(1)}, bf16[1408,128]{1,0:T(8,128)(2,1)S(1)}, u32[]{:S(2)}, u32[]{:S(2)}) %collective-permute-start.13) | collective-permute-done | bytes 360480 | tf_op jit(solution)/shard_map/ppermute | solution.py:24
  240.9 2.2 all_gather.21
  243.2 10.5 %all-gather.9.cloned.1.call-done = bf16[1024,1408]{1,0:T(8,128)(2,1)} async-done(((bf16[128,1408]{1,0:T(8,128)(2,1)}), bf16[1024,1408]{1,0:T(8,128)(2,1)}) %all-gather.9.cloned.1.call-update) | async-done | bytes 2883600 | tf_op jit(solution)/shard_map/all_gather | solution.py:43
  253.7 4.0 %fusion.16 = f32[256,1408]{1,0:T(8,128)} fusion(bf16[1024,1408]{1,0:T(8,128)(2,1)} %all-gather.9.cloned.1.call-done, bf16[256,1024]{1,0:T(8,128)(2,1)S(1)} %all_gather.21, f32[1024]{0:T(1024)S(1)} %copy-done.3, f32[256]{0:T(256)S(1)} %add_rsqrt_fusion.1), kind=kOutput, calls=%fused_computation.27 | convolution fusion | flops 739246080 | bytes 4854784 | tf_op jit(solution)/shard_map/dot_general | solution.py:63
  257.7 54.6 %all-gather.11.cloned.1.call-done = bf16[1024,1408]{1,0:T(8,128)(2,1)} async-done(((bf16[128,1408]{1,0:T(8,128)(2,1)}), bf16[1024,1408]{1,0:T(8,128)(2,1)}) %all-gather.11.cloned.1.call-update) | async-done | bytes 2883600 | tf_op jit(solution)/shard_map/all_gather | solution.py:43
  312.3 5.0 %convolution_convert_fusion = bf16[256,1024]{1,0:T(8,128)(2,1)} fusion(bf16[1408,1024]{1,0:T(8,128)(2,1)S(1)} %constant_dynamic-update-slice_fusion, bf16[1024,1408]{1,0:T(8,128)(2,1)} %all-gather.11.cloned.1.call-done, f32[256,1408]{1,0:T(8,128)} %fusion.16, bf16[256,1024]{1,0:T(8,128)(2,1)S(1)} %all_gather.21, f32[1024]{0:T(1024)S(1)} %copy-done.3, ...), kind=kOutput, calls=%fused_computation.6 | convolution fusion | flops 1479868416 | bytes 8262656 | tf_op jit(solution)/shard_map/dot_general | solution.py:111
  317.3 6.7 %reduce-scatter.5.cloned.1.call-done = bf16[256,512]{1,0:T(8,128)(2,1)} async-done(((bf16[256,1024]{1,0:T(8,128)(2,1)}), bf16[256,512]{1,0:T(8,128)(2,1)}) %reduce-scatter.5.cloned.1.call-update) | async-done | bytes 262160 | tf_op jit(solution)/shard_map/reduce_scatter | solution.py:112
  325.1 2.5 psum.7
  (58 shorter events, 21.0 us)
Async XLA Ops:
  6.5 94.0 %all-gather.5.cloned.1.call-start = ((), (), s32[]{:S(2)}) async-start(), calls=%async_computation.2 | async-start | bytes 3244032 | tf_op jit(solution)/shard_map/all_gather | solution.py:43
  7.3 151.6 %all-gather.7.cloned.1.call-start = ((), (), s32[]{:S(2)}) async-start(), calls=%async_computation.3 | async-start | bytes 3244032 | tf_op jit(solution)/shard_map/all_gather | solution.py:43
  8.0 231.7 %reduce-scatter.3.cloned.1.call-start = ((), (), s32[]{:S(2)}) async-start(), calls=%async_computation.4 | async-start | bytes 786432 | tf_op jit(solution)/shard_map/reduce_scatter | solution.py:101
  8.1 22.6 %collective-permute-start = (bf16[1408,128]{1,0:T(8,128)(2,1)}, bf16[1408,128]{1,0:T(8,128)(2,1)}, u32[]{:S(2)}, u32[]{:S(2)}) collective-permute-start(bf16[1408,128]{1,0:T(8,128)(2,1)} %param.16), channel_id=1, source_target_pairs={{0,2},{2,4},{4,6},{6,8},{8,10},{10,12},{12,14},{14,0},{1,3},{3,5},... | collective-permute-start | bytes 1081352 | tf_op jit(solution)/shard_map/ppermute | solution.py:24
  11.1 22.1 %collective-permute-start.1 = (bf16[1408,128]{1,0:T(8,128)(2,1)}, bf16[1408,128]{1,0:T(8,128)(2,1)}, u32[]{:S(2)}, u32[]{:S(2)}) collective-permute-start(bf16[1408,128]{1,0:T(8,128)(2,1)} %param.16), channel_id=1, source_target_pairs={{0,14},{2,0},{4,2},{6,4},{8,6},{10,8},{12,10},{14,12},{1,15},{3,1}... | collective-permute-start | bytes 1081352 | tf_op jit(solution)/shard_map/ppermute | solution.py:29
  14.2 4.8 %copy-start.1 = (bf16[1408,128]{1,0:T(8,128)(2,1)S(1)}, bf16[1408,128]{1,0:T(8,128)(2,1)}, u32[]{:S(2)}) copy-start(bf16[1408,128]{1,0:T(8,128)(2,1)} %param.16) | copy-start | bytes 1081348
  30.7 18.0 %collective-permute-start.2 = (bf16[1408,128]{1,0:T(8,128)(2,1)}, bf16[1408,128]{1,0:T(8,128)(2,1)S(1)}, u32[]{:S(2)}, u32[]{:S(2)}) collective-permute-start(bf16[1408,128]{1,0:T(8,128)(2,1)} %collective-permute-done), channel_id=1, source_target_pairs={{0,2},{2,4},{4,6},{6,8},{8,10},{10,12},{12,14},{14,0},{1,3},{3,5},... | collective-permute-start | bytes 1081352 | tf_op jit(solution)/shard_map/ppermute | solution.py:24
  33.2 17.2 %collective-permute-start.3 = (bf16[1408,128]{1,0:T(8,128)(2,1)}, bf16[1408,128]{1,0:T(8,128)(2,1)S(1)}, u32[]{:S(2)}, u32[]{:S(2)}) collective-permute-start(bf16[1408,128]{1,0:T(8,128)(2,1)} %collective-permute-done.1), channel_id=1, source_target_pairs={{0,14},{2,0},{4,2},{6,4},{8,6},{10,8},{12,10},{14,12},{1,15},{3,1}... | collective-permute-start | bytes 1081352 | tf_op jit(solution)/shard_map/ppermute | solution.py:29
  48.7 24.5 %collective-permute-start.4 = (bf16[1408,128]{1,0:T(8,128)(2,1)S(1)}, bf16[1408,128]{1,0:T(8,128)(2,1)S(1)}, u32[]{:S(2)}, u32[]{:S(2)}) collective-permute-start(bf16[1408,128]{1,0:T(8,128)(2,1)S(1)} %collective-permute-done.2), channel_id=1, source_target_pairs={{0,2},{2,4},{4,6},{6,8},{8,10},{10,12},{12,14},{14,0},{1,3},{3,5},... | collective-permute-start | bytes 1081352 | tf_op jit(solution)/shard_map/ppermute | solution.py:24
  50.4 27.7 %collective-permute-start.5 = (bf16[1408,128]{1,0:T(8,128)(2,1)S(1)}, bf16[1408,128]{1,0:T(8,128)(2,1)S(1)}, u32[]{:S(2)}, u32[]{:S(2)}) collective-permute-start(bf16[1408,128]{1,0:T(8,128)(2,1)S(1)} %collective-permute-done.3), channel_id=1, source_target_pairs={{0,14},{2,0},{4,2},{6,4},{8,6},{10,8},{12,10},{14,12},{1,15},{3,1}... | collective-permute-start | bytes 1081352 | tf_op jit(solution)/shard_map/ppermute | solution.py:29
  73.2 14.1 %collective-permute-start.6 = (bf16[1408,128]{1,0:T(8,128)(2,1)S(1)}, bf16[1408,128]{1,0:T(8,128)(2,1)S(1)}, u32[]{:S(2)}, u32[]{:S(2)}) collective-permute-start(bf16[1408,128]{1,0:T(8,128)(2,1)S(1)} %collective-permute-done.4), channel_id=1, source_target_pairs={{0,2},{2,4},{4,6},{6,8},{8,10},{10,12},{12,14},{14,0},{1,3},{3,5},... | collective-permute-start | bytes 1081352 | tf_op jit(solution)/shard_map/ppermute | solution.py:24
  163.7 6.4 %copy-start.2 = (bf16[1408,128]{1,0:T(8,128)(2,1)S(1)}, bf16[1408,128]{1,0:T(8,128)(2,1)}, u32[]{:S(2)}) copy-start(bf16[1408,128]{1,0:T(8,128)(2,1)} %param.20) | copy-start | bytes 1081348
  163.7 90.0 %all-gather.9.cloned.1.call-start = ((), (), s32[]{:S(2)}) async-start(), calls=%async_computation.5 | async-start | bytes 3244032 | tf_op jit(solution)/shard_map/all_gather | solution.py:43
  164.3 148.0 %all-gather.11.cloned.1.call-start = ((), (), s32[]{:S(2)}) async-start(), calls=%async_computation.6 | async-start | bytes 3244032 | tf_op jit(solution)/shard_map/all_gather | solution.py:43
  164.9 159.1 %reduce-scatter.5.cloned.1.call-start = ((), (), s32[]{:S(2)}) async-start(), calls=%async_computation.7 | async-start | bytes 786432 | tf_op jit(solution)/shard_map/reduce_scatter | solution.py:112
  164.9 14.6 %collective-permute-start.7 = (bf16[1408,128]{1,0:T(8,128)(2,1)}, bf16[1408,128]{1,0:T(8,128)(2,1)}, u32[]{:S(2)}, u32[]{:S(2)}) collective-permute-start(bf16[1408,128]{1,0:T(8,128)(2,1)} %param.20), channel_id=1, source_target_pairs={{0,2},{2,4},{4,6},{6,8},{8,10},{10,12},{12,14},{14,0},{1,3},{3,5},... | collective-permute-start | bytes 1081352 | tf_op jit(solution)/shard_map/ppermute | solution.py:24
  165.5 17.4 %collective-permute-start.8 = (bf16[1408,128]{1,0:T(8,128)(2,1)}, bf16[1408,128]{1,0:T(8,128)(2,1)}, u32[]{:S(2)}, u32[]{:S(2)}) collective-permute-start(bf16[1408,128]{1,0:T(8,128)(2,1)} %param.20), channel_id=1, source_target_pairs={{0,14},{2,0},{4,2},{6,4},{8,6},{10,8},{12,10},{14,12},{1,15},{3,1}... | collective-permute-start | bytes 1081352 | tf_op jit(solution)/shard_map/ppermute | solution.py:29
  170.1 69.6 %copy-start = (bf16[128,1024]{1,0:T(8,128)(2,1)S(1)}, bf16[128,1024]{1,0:T(8,128)(2,1)}, u32[]{:S(2)}) copy-start(bf16[128,1024]{1,0:T(8,128)(2,1)} %param.11) | copy-start | bytes 786436
  179.6 18.2 %collective-permute-start.9 = (bf16[1408,128]{1,0:T(8,128)(2,1)}, bf16[1408,128]{1,0:T(8,128)(2,1)S(1)}, u32[]{:S(2)}, u32[]{:S(2)}) collective-permute-start(bf16[1408,128]{1,0:T(8,128)(2,1)} %collective-permute-done.7), channel_id=1, source_target_pairs={{0,2},{2,4},{4,6},{6,8},{8,10},{10,12},{12,14},{14,0},{1,3},{3,5},... | collective-permute-start | bytes 1081352 | tf_op jit(solution)/shard_map/ppermute | solution.py:24
  182.9 20.7 %collective-permute-start.10 = (bf16[1408,128]{1,0:T(8,128)(2,1)}, bf16[1408,128]{1,0:T(8,128)(2,1)S(1)}, u32[]{:S(2)}, u32[]{:S(2)}) collective-permute-start(bf16[1408,128]{1,0:T(8,128)(2,1)} %collective-permute-done.8), channel_id=1, source_target_pairs={{0,14},{2,0},{4,2},{6,4},{8,6},{10,8},{12,10},{14,12},{1,15},{3,1}... | collective-permute-start | bytes 1081352 | tf_op jit(solution)/shard_map/ppermute | solution.py:29
  187.1 66.6 %copy-start.3 = (f32[1024]{0:T(1024)S(1)}, f32[1024]{0:T(1024)}, u32[]{:S(2)}) copy-start(f32[1024]{0:T(1024)} %param.17) | copy-start | bytes 12292
  197.8 18.7 %collective-permute-start.11 = (bf16[1408,128]{1,0:T(8,128)(2,1)S(1)}, bf16[1408,128]{1,0:T(8,128)(2,1)S(1)}, u32[]{:S(2)}, u32[]{:S(2)}) collective-permute-start(bf16[1408,128]{1,0:T(8,128)(2,1)S(1)} %collective-permute-done.9), channel_id=1, source_target_pairs={{0,2},{2,4},{4,6},{6,8},{8,10},{10,12},{12,14},{14,0},{1,3},{3,5},... | collective-permute-start | bytes 1081352 | tf_op jit(solution)/shard_map/ppermute | solution.py:24
  203.6 26.7 %collective-permute-start.12 = (bf16[1408,128]{1,0:T(8,128)(2,1)S(1)}, bf16[1408,128]{1,0:T(8,128)(2,1)S(1)}, u32[]{:S(2)}, u32[]{:S(2)}) collective-permute-start(bf16[1408,128]{1,0:T(8,128)(2,1)S(1)} %collective-permute-done.10), channel_id=1, source_target_pairs={{0,14},{2,0},{4,2},{6,4},{8,6},{10,8},{12,10},{14,12},{1,15},{3,1}... | collective-permute-start | bytes 1081352 | tf_op jit(solution)/shard_map/ppermute | solution.py:29
  216.5 23.1 %collective-permute-start.13 = (bf16[1408,128]{1,0:T(8,128)(2,1)S(1)}, bf16[1408,128]{1,0:T(8,128)(2,1)S(1)}, u32[]{:S(2)}, u32[]{:S(2)}) collective-permute-start(bf16[1408,128]{1,0:T(8,128)(2,1)S(1)} %collective-permute-done.11), channel_id=1, source_target_pairs={{0,2},{2,4},{4,6},{6,8},{8,10},{10,12},{12,14},{14,0},{1,3},{3,5},... | collective-permute-start | bytes 1081352 | tf_op jit(solution)/shard_map/ppermute | solution.py:24
  257.7 69.9 %copy-start.4 = (f32[512]{0:T(512)S(1)}, f32[512]{0:T(512)}, u32[]{:S(2)}) copy-start(f32[512]{0:T(512)} %param.21) | copy-start | bytes 6148
Sparse Core Ops, SparseCore 0:
  9.5 90.9 all-gather.4
  102.7 56.0 all-gather.6
  163.8 6.5 reduce-scatter.2
  172.5 81.2 all-gather.8
  255.8 56.5 all-gather.10
  317.4 6.5 reduce-scatter.4
